TPU v7x, 32 devices: a whole 2x2x4 slice. The times are simulated.
32 devices in a mesh: fs: 16 (over z, y, x), tp: 2 (over core).
Axes of the slice: x: 2, y: 2, z: 4, core: 2. Of those that a mesh axis runs over, the one named last changes fastest.
Arguments:
- tokens: bfloat16 [4096, 2048], P('fs'), may hold values from -6 to 6
- routes: int32 [4096, 6], P('fs'), may hold values from 0 to 15, all different within a row; in each aligned block of 256 rows (0 to 255, 256 to 511, ...) at most 160 rows name the same one
- route_weights: float32 [4096, 6], P('fs'), may hold values from 0.1 to 1
- norm_gain: float32 [2048], P('fs'), may hold values from 0.1 to 1.9
- expert_gate: float32 [16, 2048, 1024], P(None, 'fs', 'tp'), may hold values from -0.125 to 0.125
- expert_up: float32 [16, 2048, 1024], P(None, 'fs', 'tp'), may hold values from -0.125 to 0.125
- expert_down: float32 [16, 2048, 1024], P(None, 'fs', 'tp'), may hold values from -0.1875 to 0.1875
- shared_gate: float32 [2048, 1024], P('fs', 'tp'), may hold values from -0.125 to 0.125
- shared_up: float32 [2048, 1024], P('fs', 'tp'), may hold values from -0.125 to 0.125
- shared_down: float32 [2048, 1024], P('fs', 'tp'), may hold values from -0.1875 to 0.1875
Outputs:
- layer_output: bfloat16 [4096, 2048], P('fs', 'tp')
- sample_gate: bfloat16 [16, 2048, 1024], P('fs', None, 'tp')
- sample_up: bfloat16 [16, 2048, 1024], P('fs', None, 'tp')
- sample_down: bfloat16 [16, 2048, 1024], P('fs', None, 'tp')
- common_gate: bfloat16 [2048, 1024], P(None, 'tp')
- common_up: bfloat16 [2048, 1024], P(None, 'tp')
- common_down: bfloat16 [2048, 1024], P(None, 'tp')
Inputs may be any that keep to these rules, and one draw needn't show every extreme that they name: `routes`: each row names 6 different experts. In each aligned block of 256 rows (the rows of one index of fs) no expert is named by more than 160 rows, a bound that some expert reaches in some blocks.
All inputs are finite; a program needn't handle non-finite values.
Results may differ from a plain program's by a relative error of at most 0.015.
Values may be sent and summed in bfloat16 or wider, within the bound.
A program may use at most 128 MiB of HBM per device.

v0:
```python
import jax
import jax.numpy as jnp
from jax import lax
from jax.sharding import PartitionSpec as P

EPSILON = 1e-06


def normalize(tokens):
    values = tokens.astype(jnp.float32)
    scale = lax.rsqrt(jnp.mean(values * values, axis=-1, keepdims=True) + EPSILON)
    return (values * scale).astype(jnp.bfloat16)


def slot_table(routes, experts, capacity):
    flat_route = routes.reshape(-1)
    member = (flat_route[:, None] == jnp.arange(experts, dtype=jnp.int32)[None, :]).astype(
        jnp.int32
    )
    before = jnp.sum((jnp.cumsum(member, axis=0) - member) * member, axis=1)
    return flat_route * capacity + before


def body(
    tokens,
    routes,
    route_weights,
    norm_gain,
    expert_gate,
    expert_up,
    expert_down,
    shared_gate,
    shared_up,
    shared_down,
):
    gain_rows = norm_gain[None, :, None]
    rounded = (
        (expert_gate * gain_rows).astype(jnp.bfloat16),
        (expert_up * gain_rows).astype(jnp.bfloat16),
        expert_down.astype(jnp.bfloat16),
    )
    sample_gate, sample_up, sample_down = (
        lax.all_to_all(rounded[0], "fs", split_axis=0, concat_axis=1, tiled=True),
        lax.all_to_all(rounded[1], "fs", split_axis=0, concat_axis=1, tiled=True),
        lax.all_to_all(rounded[2], "fs", split_axis=0, concat_axis=1, tiled=True),
    )
    gate_rows = sample_gate[0]
    up_rows = sample_up[0]
    down_rows = sample_down[0]
    normed = normalize(tokens)
    tok_rows, width = normed.shape
    picks = routes.shape[1]
    experts = expert_gate.shape[0]
    tp_count = lax.axis_size("tp")
    capacity = min(tok_rows, tp_count * max(1, tok_rows * picks * 5 // (3 * experts * tp_count)))
    slots = slot_table(routes, experts, capacity)
    sources = (
        jnp.full((experts * capacity,), tok_rows, jnp.int32)
        .at[slots]
        .set(jnp.arange(tok_rows * picks, dtype=jnp.int32) // picks)
    )
    padded = jnp.concatenate([normed, jnp.zeros((1, width), jnp.bfloat16)], axis=0)
    outgoing = padded[sources].reshape(experts, capacity, width)
    shared_rounded = (
        (shared_gate * norm_gain[:, None]).astype(jnp.bfloat16),
        (shared_up * norm_gain[:, None]).astype(jnp.bfloat16),
        shared_down.astype(jnp.bfloat16),
    )
    common_gate, common_up, common_down = (
        lax.all_gather(shared_rounded[0], "fs", axis=0, tiled=True),
        lax.all_gather(shared_rounded[1], "fs", axis=0, tiled=True),
        lax.all_gather(shared_rounded[2], "fs", axis=0, tiled=True),
    )
    shared_gate_act = jnp.dot(normed, common_gate, preferred_element_type=jnp.float32)
    shared_up_act = jnp.dot(normed, common_up, preferred_element_type=jnp.float32)
    shared_hidden = (jax.nn.silu(shared_gate_act) * shared_up_act).astype(jnp.bfloat16)
    shared_terms = jnp.einsum(
        "th,dh->td", shared_hidden, common_down, preferred_element_type=jnp.float32
    )
    share = capacity // tp_count
    whole_gate, whole_up, whole_down = (
        lax.all_gather(gate_rows, "tp", axis=1, tiled=True),
        lax.all_gather(up_rows, "tp", axis=1, tiled=True),
        lax.all_gather(down_rows, "tp", axis=1, tiled=True),
    )
    own_share = lax.dynamic_slice_in_dim(outgoing, lax.axis_index("tp") * share, share, 1)
    block = lax.all_to_all(own_share, "fs", split_axis=0, concat_axis=0, tiled=True)
    flat = block.reshape(-1, width)
    gate = jnp.dot(flat, whole_gate, preferred_element_type=jnp.float32)
    upward = jnp.dot(flat, whole_up, preferred_element_type=jnp.float32)
    hidden = (jax.nn.silu(gate) * upward).astype(jnp.bfloat16)
    parts = jnp.einsum(
        "rbf,dbf->rbd",
        hidden.reshape(flat.shape[0], tp_count, -1),
        whole_down.reshape(width, tp_count, -1),
        preferred_element_type=jnp.float32,
    ).astype(jnp.bfloat16)
    parts = lax.optimization_barrier(parts)
    total = jnp.sum(parts.astype(jnp.float32), axis=1).astype(jnp.bfloat16)
    results = total.reshape(block.shape[0], block.shape[1], width)
    back = lax.all_to_all(results, "fs", split_axis=0, concat_axis=0, tiled=True).reshape(
        experts * share, width
    )
    position = slots % capacity
    owner = position // share
    local = slots // capacity * share + position % share
    taken = back[local].astype(jnp.float32).reshape(tok_rows, picks, width)
    keep = (owner == lax.axis_index("tp")).astype(jnp.float32).reshape(tok_rows, picks)
    routed_part = jnp.sum(taken * (route_weights * keep)[:, :, None], axis=1)
    shared_part = lax.optimization_barrier(shared_terms.astype(jnp.bfloat16)).astype(jnp.float32)
    layer_output = lax.psum_scatter(
        (routed_part + shared_part).astype(jnp.bfloat16), "tp", scatter_dimension=1, tiled=True
    )
    return (layer_output, sample_gate, sample_up, sample_down, common_gate, common_up, common_down)


def solution(mesh):
    return jax.shard_map(
        body,
        mesh=mesh,
        in_specs=(
            P("fs", None),
            P("fs", None),
            P("fs", None),
            P("fs"),
            P(None, "fs", "tp"),
            P(None, "fs", "tp"),
            P(None, "fs", "tp"),
            P("fs", "tp"),
            P("fs", "tp"),
            P("fs", "tp"),
        ),
        out_specs=(
            P("fs", "tp"),
            P("fs", None, "tp"),
            P("fs", None, "tp"),
            P("fs", None, "tp"),
            P(None, "tp"),
            P(None, "tp"),
            P(None, "tp"),
        ),
        check_vma=False,
    )
```

profile of v0, /device:TPU:0, one launch (start us, length us, event | category | flops | bytes accessed | tf_op | source)
XLA Modules:
  0.0 618.7 jit_solution(1220370238295980275)
XLA Ops:
  7.2 6.1 multiply_convert_fusion.1
  13.3 57.0 %all_to_all.46 = bf16[16,128,512]{2,1,0:T(8,128)(2,1)} all-to-all(bf16[16,128,512]{2,1,0:T(8,128)(2,1)S(1)} %get-tuple-element.12), channel_id=1, replica_groups=mesh['fs'=16,'tp'=2] {'fs'}, dimensions={0} | all-to-all | bytes 4194304 | tf_op jit(solution)/shard_map/all_to_all | solution.py:43
  70.3 3.9 all-to-all-start.2
  74.3 3.8 convert_element_type.70
  78.1 38.7 %all-to-all-done.2 = bf16[16,128,512]{2,1,0:T(8,128)(2,1)S(1)} async-done(((bf16[16,128,512]{2,1,0:T(8,128)(2,1)}), bf16[16,128,512]{2,1,0:T(8,128)(2,1)S(1)}, u32[]{:S(2)}, u32[]{:S(2)}) %all-to-all-start.2) | async-done | bytes 2097184 | tf_op jit(solution)/shard_map/all_to_all | solution.py:44
  116.8 9.9 %all-to-all-start.3 = ((bf16[16,128,512]{2,1,0:T(8,128)(2,1)}), bf16[16,128,512]{2,1,0:T(8,128)(2,1)}, u32[]{:S(2)}, u32[]{:S(2)}) async-start(bf16[16,128,512]{2,1,0:T(8,128)(2,1)} %convert_element_type.70), calls=%async_computation.3 | async-start | bytes 4194304 | tf_op jit(solution)/shard_map/all_to_all | solution.py:45
  126.7 0.0 all-gather.7.cloned.1.call-start
  126.8 0.1 copy.30
  126.9 0.1 eq.39
  127.1 0.1 eq.35
  127.2 0.2 all-gather.7.cloned.1.call-update
  127.5 4.6 reduce-window.6
  132.0 0.4 slice_reduce_fusion
  132.5 0.2 reduce-window.9
  132.6 0.1 copy.29
  132.8 0.1 mul.113
  132.9 0.3 fusion.1
  133.2 0.2 fusion.2
  133.5 0.1 concatenate.3
  133.6 0.1 broadcast_add_fusion
  133.7 0.1 fusion.13
  133.8 0.1 fusion.22
  133.9 6.2 %scatter_custom_fusion = s32[2560]{0:T(1024)S(1)} fusion(s32[1536]{0:T(1024)S(1)} %get-tuple-element.8, s32[1536]{0:T(1024)S(1)} %add_select_fusion.2, s32[]{:T(128)} %constant.63.clone.1), kind=kCustom, calls=%fused_computation.62 | custom fusion | bytes 10244 | tf_op jit(solution)/shard_map/scatter | solution.py:60
  140.1 10.8 %gather_fusion = bf16[2560,2048]{1,0:T(8,128)(2,1)} fusion(bf16[257,2048]{1,0:T(8,128)(2,1)S(1)} %concatenate.3, s32[3072]{0:T(1024)S(1)} %pad_clamp_fusion), kind=kCustom, calls=%fused_computation | custom fusion | bytes 20981760 | tf_op jit(solution)/shard_map/gather | solution.py:63
  150.9 5.7 constant_dynamic-slice_fusion
  156.6 12.7 %all-to-all-done.3 = bf16[16,128,512]{2,1,0:T(8,128)(2,1)} async-done(((bf16[16,128,512]{2,1,0:T(8,128)(2,1)}), bf16[16,128,512]{2,1,0:T(8,128)(2,1)}, u32[]{:S(2)}, u32[]{:S(2)}) %all-to-all-start.3) | async-done | bytes 2097184 | tf_op jit(solution)/shard_map/all_to_all | solution.py:45
  169.3 9.8 %all-to-all-start = ((bf16[16,80,2048]{2,1,0:T(8,128)(2,1)}), bf16[16,80,2048]{2,1,0:T(8,128)(2,1)}, u32[]{:S(2)}, u32[]{:S(2)}) async-start(bf16[16,80,2048]{2,1,0:T(8,128)(2,1)} %constant_dynamic-slice_fusion), calls=%async_computation | async-start | bytes 10485760 | tf_op jit(solution)/shard_map/all_to_all | solution.py:87
  179.2 0.0 all-gather.9.cloned.1.call-start
  179.3 0.7 all-gather.9.cloned.1.call-update
  179.9 0.0 all-gather.11.cloned.1.call-start
  180.0 3.9 copy.39
  183.9 0.2 all-gather.13.cloned.1.call-start
  184.2 0.8 multiply_convert_fusion.4
  185.0 0.0 all-gather.7.cloned.1.call-done
  185.0 99.7 %all-to-all-done = bf16[16,80,2048]{2,1,0:T(8,128)(2,1)} async-done(((bf16[16,80,2048]{2,1,0:T(8,128)(2,1)}), bf16[16,80,2048]{2,1,0:T(8,128)(2,1)}, u32[]{:S(2)}, u32[]{:S(2)}) %all-to-all-start) | async-done | bytes 5242912 | tf_op jit(solution)/shard_map/all_to_all | solution.py:87
  284.7 10.6 %fusion.27 = f32[1280,1024]{0,1:T(8,128)} fusion(bf16[1280,2048]{1,0:T(8,128)(2,1)} %bitcast.2, bf16[2048,1024]{1,0:T(8,128)(2,1)} %all-gather.7.cloned.1.call-done), kind=kOutput, calls=%fused_computation.68 | convolution fusion | flops 5368709120 | bytes 14680064 | tf_op jit(solution)/shard_map/dot_general | solution.py:89
  295.3 11.6 %multiply_convert_fusion = bf16[1280,1024]{0,1:T(8,128)(2,1)} fusion(f32[1280,1024]{0,1:T(8,128)} %fusion.27, bf16[1280,2048]{1,0:T(8,128)(2,1)} %bitcast.2, bf16[2048,1024]{1,0:T(8,128)(2,1)} %all-gather.9.cloned.1.call-done), kind=kOutput, calls=%fused_computation.6 | convolution fusion | flops 5376573440 | bytes 17301504 | tf_op jit(solution)/shard_map/dot_general | solution.py:90
  306.9 10.9 %fusion = bf16[1280,2,2048]{2,0,1:T(8,128)(2,1)} fusion(bf16[1280,2,512]{0,2,1:T(8,128)(2,1)} %bitcast.52, bf16[2048,2,512]{0,2,1:T(8,128)(2,1)} %bitcast.51), kind=kOutput, calls=%fused_computation.5 | convolution fusion | flops 5373952000 | bytes 17301504 | tf_op jit(solution)/shard_map/rbf,dbf->rbd/dot_general | solution.py:92
  317.8 11.2 %reduce_sum.46 = bf16[1280,2048]{1,0:T(8,128)(2,1)} reduce(bf16[1280,2,2048]{2,0,1:T(8,128)(2,1)} %fusion, bf16[]{:T(256)} %constant.62.clone.1), dimensions={1}, to_apply=%region_5.6 | reduce | flops 2621440 | bytes 15728642 | tf_op jit(solution)/shard_map/reduce_sum | solution.py:99
  329.0 35.7 %all-to-all-start.4 = ((bf16[16,80,2048]{2,1,0:T(8,128)(2,1)}), bf16[16,80,2048]{2,1,0:T(8,128)(2,1)}, u32[]{:S(2)}, u32[]{:S(2)}) async-start(bf16[16,80,2048]{2,1,0:T(8,128)(2,1)} %bitcast.44), calls=%async_computation.4 | async-start | bytes 10485760 | tf_op jit(solution)/shard_map/all_to_all | solution.py:101
  364.8 0.0 all-gather.15.cloned.1.call-start
  364.8 0.5 all-gather.15.cloned.1.call-update
  365.4 0.0 all-gather.17.cloned.1.call-start
  365.4 0.7 convert_element_type.78
  366.1 0.0 reduce-scatter.2.cloned.1.call-start
  366.2 0.1 reduce_sum.47
  366.3 0.1 copy.35
  366.4 0.1 copy.36
  366.6 2.3 fusion.28
  368.9 120.3 %all-gather.15.cloned.1.call-done = bf16[2048,512]{1,0:T(8,128)(2,1)} async-done(((bf16[128,512]{1,0:T(8,128)(2,1)}), bf16[2048,512]{1,0:T(8,128)(2,1)}) %all-gather.15.cloned.1.call-update) | async-done | bytes 2097168 | tf_op jit(solution)/shard_map/all_gather | solution.py:71
  489.2 62.3 %all-gather.17.cloned.1.call-done = bf16[2048,512]{1,0:T(8,128)(2,1)} async-done(((bf16[128,512]{1,0:T(8,128)(2,1)}), bf16[2048,512]{1,0:T(8,128)(2,1)}) %all-gather.17.cloned.1.call-update) | async-done | bytes 2097168 | tf_op jit(solution)/shard_map/all_gather | solution.py:72
  551.5 3.6 convolution_convert_fusion.1
  555.1 16.1 %gather_fusion.1 = bf16[1536,2048]{1,0:T(8,128)(2,1)} fusion(bf16[1280,2048]{1,0:T(8,128)(2,1)} %bitcast.10, s32[2048]{0:T(1024)S(1)} %pad_clamp_fusion.1), kind=kCustom, calls=%fused_computation.1 | custom fusion | bytes 12589056 | tf_op jit(solution)/shard_map/gather | solution.py:107
  571.2 11.7 %reshape.194 = f32[256,6,2048]{2,1,0:T(8,128)} reshape(bf16[1536,2048]{1,0:T(8,128)(2,1)} %gather_fusion.1) | data formatting | bytes 18874368 | tf_op jit(solution)/shard_map/convert_element_type | solution.py:107
  582.9 9.4 %multiply_reduce_fusion = f32[256,2048]{1,0:T(8,128)S(1)} fusion(f32[256,6,2048]{2,1,0:T(8,128)} %reshape.194, f32[256,6]{1,0:T(8,128)S(1)} %copy.36), kind=kLoop, calls=%fused_computation.3 | loop fusion | flops 5767168 | bytes 14686208 | tf_op jit(solution)/shard_map/reduce_sum | solution.py:109
  592.3 1.3 add_convert_fusion
  593.7 7.3 %reduce-scatter.2.cloned.1.call-done = bf16[256,1024]{1,0:T(8,128)(2,1)} async-done(((bf16[256,2048]{1,0:T(8,128)(2,1)}), bf16[256,1024]{1,0:T(8,128)(2,1)}) %reduce-scatter.2.cloned.1.call-update) | async-done | bytes 524304 | tf_op jit(solution)/shard_map/reduce_scatter | solution.py:111
  601.0 1.3 copy.48
  602.3 1.0 copy-done.2
  603.4 1.3 copy.49
  604.7 3.2 copy.50
  607.9 1.3 copy.51
  609.2 1.3 copy.52
  610.5 1.3 copy.53
  (41 shorter events, 0.2 us)
Async XLA Ops:
  70.3 46.5 %all-to-all-start.2 = ((bf16[16,128,512]{2,1,0:T(8,128)(2,1)}), bf16[16,128,512]{2,1,0:T(8,128)(2,1)S(1)}, u32[]{:S(2)}, u32[]{:S(2)}) async-start(bf16[16,128,512]{2,1,0:T(8,128)(2,1)} %get-tuple-element.11), calls=%async_computation.2 | async-start | bytes 4194304 | tf_op jit(solution)/shard_map/all_to_all | solution.py:44
  74.3 52.5 %copy-start.10 = (s32[256,6]{0,1:T(8,128)S(1)}, s32[256,6]{0,1:T(8,128)}, u32[]{:S(2)}) copy-start(s32[256,6]{0,1:T(8,128)} %param.11) | copy-start | bytes 18436
  78.1 54.8 %copy-start.3 = (bf16[256,2048]{1,0:T(8,128)(2,1)S(1)}, bf16[256,2048]{1,0:T(8,128)(2,1)}, u32[]{:S(2)}) copy-start(bf16[256,2048]{1,0:T(8,128)(2,1)} %param.10) | copy-start | bytes 3145732
  116.8 16.4 %copy-start.1 = (bf16[16,128,512]{2,1,0:T(8,128)(2,1)}, bf16[16,128,512]{2,1,0:T(8,128)(2,1)S(1)}, u32[]{:S(2)}) copy-start(bf16[16,128,512]{2,1,0:T(8,128)(2,1)S(1)} %all-to-all-done.2) | copy-start | bytes 6291460
  116.8 52.5 %all-to-all-start.3 = ((bf16[16,128,512]{2,1,0:T(8,128)(2,1)}), bf16[16,128,512]{2,1,0:T(8,128)(2,1)}, u32[]{:S(2)}, u32[]{:S(2)}) async-start(bf16[16,128,512]{2,1,0:T(8,128)(2,1)} %convert_element_type.70), calls=%async_computation.3 | async-start | bytes 4194304 | tf_op jit(solution)/shard_map/all_to_all | solution.py:45
  126.7 58.3 %all-gather.7.cloned.1.call-start = ((), (), s32[]{:S(2)}) async-start(), calls=%async_computation.6 | async-start | bytes 6291456 | tf_op jit(solution)/shard_map/all_gather | solution.py:82
  169.3 115.4 %all-to-all-start = ((bf16[16,80,2048]{2,1,0:T(8,128)(2,1)}), bf16[16,80,2048]{2,1,0:T(8,128)(2,1)}, u32[]{:S(2)}, u32[]{:S(2)}) async-start(bf16[16,80,2048]{2,1,0:T(8,128)(2,1)} %constant_dynamic-slice_fusion), calls=%async_computation | async-start | bytes 10485760 | tf_op jit(solution)/shard_map/all_to_all | solution.py:87
  179.2 116.1 %all-gather.9.cloned.1.call-start = ((), (), s32[]{:S(2)}) async-start(), calls=%async_computation.7 | async-start | bytes 6291456 | tf_op jit(solution)/shard_map/all_gather | solution.py:83
  179.2 4.9 copy-start.8
  179.2 4.9 copy-start.9
  179.2 4.9 copy-start.12
  179.9 126.9 %all-gather.11.cloned.1.call-start = ((), (), s32[]{:S(2)}) async-start(), calls=%async_computation.8 | async-start | bytes 6291456 | tf_op jit(solution)/shard_map/all_gather | solution.py:84
  183.9 182.7 %all-gather.13.cloned.1.call-start = ((), (), s32[]{:S(2)}) async-start(), calls=%async_computation.9 | async-start | bytes 2228224 | tf_op jit(solution)/shard_map/all_gather | solution.py:70
  329.0 36.4 %copy-start.7 = (f32[128,512]{1,0:T(8,128)S(1)}, f32[128,512]{1,0:T(8,128)}, u32[]{:S(2)}) copy-start(f32[128,512]{1,0:T(8,128)} %param.19) | copy-start | bytes 786436
  329.0 37.4 %copy-start.11 = (f32[256,6]{0,1:T(8,128)S(1)}, f32[256,6]{0,1:T(8,128)}, u32[]{:S(2)}) copy-start(f32[256,6]{0,1:T(8,128)} %param.12) | copy-start | bytes 18436
  329.0 226.1 %all-to-all-start.4 = ((bf16[16,80,2048]{2,1,0:T(8,128)(2,1)}), bf16[16,80,2048]{2,1,0:T(8,128)(2,1)}, u32[]{:S(2)}, u32[]{:S(2)}) async-start(bf16[16,80,2048]{2,1,0:T(8,128)(2,1)} %bitcast.44), calls=%async_computation.4 | async-start | bytes 10485760 | tf_op jit(solution)/shard_map/all_to_all | solution.py:101
  364.8 124.4 %all-gather.15.cloned.1.call-start = ((), (), s32[]{:S(2)}) async-start(), calls=%async_computation.10 | async-start | bytes 2228224 | tf_op jit(solution)/shard_map/all_gather | solution.py:71
  365.4 186.1 %all-gather.17.cloned.1.call-start = ((), (), s32[]{:S(2)}) async-start(), calls=%async_computation.11 | async-start | bytes 2228224 | tf_op jit(solution)/shard_map/all_gather | solution.py:72
  366.1 234.9 %reduce-scatter.2.cloned.1.call-start = ((), (), s32[]{:S(2)}) async-start(), calls=%async_computation.12 | async-start | bytes 1572864 | tf_op jit(solution)/shard_map/reduce_scatter | solution.py:111
  592.3 8.7 %copy-start = (bf16[16,128,512]{2,1,0:T(8,128)(2,1)S(1)}, bf16[16,128,512]{2,1,0:T(8,128)(2,1)}, u32[]{:S(2)}) copy-start(bf16[16,128,512]{2,1,0:T(8,128)(2,1)} %all_to_all.46) | copy-start | bytes 6291460
  601.0 2.3 copy-start.2
  603.4 4.5 copy-start.4
  604.7 4.5 copy-start.5
  607.9 2.6 copy-start.6
Sparse Core Ops, SparseCore 0:
  129.1 14.9 all-gather.6
  182.1 14.8 all-gather.8
  199.2 14.8 all-gather.10
  217.2 96.2 all-gather.12
  368.6 120.5 all-gather.14
  492.4 59.0 all-gather.16
  593.8 7.1 reduce-scatter.1
where the time goes:
time: 620 us; the launch traced here: 619 us
  waiting for transfers between devices  343 us (55%)
  local copies, waits for them, and re-layouts  66.9 us (11%)
  starting transfers between devices  59.8 us (10%)
  blocking collectives  57 us (9%)
  matrix products  39 us (6%)
  other arithmetic  38.9 us (6%)
  between operations  14.5 us (2%)
    all_gather x1, waiting for transfers between devices, body(): lax.all_gather(shared_rounded[1], 'fs', axis=0, tiled=True)  120 us
    all_to_all x1, waiting for transfers between devices, body(): lax.all_to_all(own_share, 'fs', split_axis=0, concat_axis=0, tiled=True)  99.7 us
    all_gather x1, waiting for transfers between devices, body(): lax.all_gather(shared_rounded[2], 'fs', axis=0, tiled=True)  62.3 us
    all_to_all x1, blocking collectives, body(): lax.all_to_all(rounded[0], 'fs', split_axis=0, concat_axis=1, tiled=True)  57 us
    all_to_all x1, waiting for transfers between devices, body(): lax.all_to_all(rounded[1], 'fs', split_axis=0, concat_axis=1, tiled=True)  38.7 us
    all_to_all x1, starting transfers between devices, body(): lax.all_to_all(results, 'fs', split_axis=0, concat_axis=0, tiled=True)  35.7 us
    gather x1, local copies, waits for them, and re-layouts, body(): taken = back[local].astype(jnp.float32).reshape(tok_rows, picks, width)  16.1 us
    all_to_all x1, waiting for transfers between devices, body(): lax.all_to_all(rounded[2], 'fs', split_axis=0, concat_axis=1, tiled=True)  12.7 us
  transfers between devices with their start and end apart: 11, of which 6 were waited for; matrix products, arithmetic and copies ran while one was open for 14% of the time, Pallas kernels for 0%

commit v1 on v0

v1 whole, which is shorter than its diff:
```python
import jax
import jax.numpy as jnp
from jax import lax
from jax.sharding import PartitionSpec as P

EPSILON = 1e-06


def normalize(tokens):
    values = tokens.astype(jnp.float32)
    scale = lax.rsqrt(jnp.mean(values * values, axis=-1, keepdims=True) + EPSILON)
    return (values * scale).astype(jnp.bfloat16)


def body(
    tokens,
    routes,
    route_weights,
    norm_gain,
    expert_gate,
    expert_up,
    expert_down,
    shared_gate,
    shared_up,
    shared_down,
):
    tp_count = lax.axis_size("tp")
    tp_index = lax.axis_index("tp")
    fs_count = lax.axis_size("fs")
    tok_rows, width = tokens.shape
    experts = expert_gate.shape[0]
    share = tok_rows // tp_count
    own_experts = experts // fs_count

    normed = normalize(tokens)
    own_normed = lax.dynamic_slice_in_dim(normed, tp_index * share, share, 0)
    own_routes = lax.dynamic_slice_in_dim(routes, tp_index * share, share, 0)
    own_weights = lax.dynamic_slice_in_dim(route_weights, tp_index * share, share, 0)
    member = own_routes[None, :, :] == jnp.arange(experts, dtype=jnp.int32)[:, None, None]
    dense = jnp.sum(jnp.where(member, own_weights[None, :, :], 0.0), axis=2)
    gathered = lax.all_gather(own_normed, "fs", axis=0, tiled=True)
    dense_all = lax.all_gather(dense, "fs", axis=0, tiled=False)

    gain_rows = norm_gain[None, :, None]
    rounded = (
        (expert_gate * gain_rows).astype(jnp.bfloat16),
        (expert_up * gain_rows).astype(jnp.bfloat16),
        expert_down.astype(jnp.bfloat16),
    )
    sample_gate, sample_up, sample_down = (
        lax.all_to_all(rounded[0], "fs", split_axis=0, concat_axis=1, tiled=True),
        lax.all_to_all(rounded[1], "fs", split_axis=0, concat_axis=1, tiled=True),
        lax.all_to_all(rounded[2], "fs", split_axis=0, concat_axis=1, tiled=True),
    )

    common_gate, common_up, common_down = (
        lax.all_gather((shared_gate * norm_gain[:, None]).astype(jnp.bfloat16), "fs", axis=0, tiled=True),
        lax.all_gather((shared_up * norm_gain[:, None]).astype(jnp.bfloat16), "fs", axis=0, tiled=True),
        lax.all_gather(shared_down.astype(jnp.bfloat16), "fs", axis=0, tiled=True),
    )
    shared_gate_act = jnp.dot(normed, common_gate, preferred_element_type=jnp.float32)
    shared_up_act = jnp.dot(normed, common_up, preferred_element_type=jnp.float32)
    shared_hidden = (jax.nn.silu(shared_gate_act) * shared_up_act).astype(jnp.bfloat16)
    shared_part = jnp.einsum(
        "th,dh->td", shared_hidden, common_down, preferred_element_type=jnp.float32
    ).astype(jnp.bfloat16)
    shared_parts = lax.all_to_all(
        shared_part.reshape(tok_rows, tp_count, width // tp_count).transpose(1, 0, 2),
        "tp",
        split_axis=0,
        concat_axis=0,
        tiled=True,
    )
    shared_sum = jnp.sum(shared_parts.astype(jnp.float32), axis=0)

    scale_all = lax.dynamic_slice_in_dim(
        dense_all, lax.axis_index("fs") * own_experts, own_experts, 1
    )
    total = None
    for expert in range(own_experts):
        scale = scale_all[:, expert, :].reshape(-1)[:, None]
        for shift in range(tp_count):
            gate_w, up_w, down_w = (
                sample_gate[expert],
                sample_up[expert],
                sample_down[expert],
            )
            if shift:
                ring = [(i, (i + shift) % tp_count) for i in range(tp_count)]
                gate_w, up_w, down_w = (
                    lax.ppermute(gate_w, "tp", ring),
                    lax.ppermute(up_w, "tp", ring),
                    lax.ppermute(down_w, "tp", ring),
                )
            gate = jnp.dot(gathered, gate_w, preferred_element_type=jnp.float32)
            upward = jnp.dot(gathered, up_w, preferred_element_type=jnp.float32)
            hidden = (jax.nn.silu(gate) * upward * scale).astype(jnp.bfloat16)
            part = jnp.einsum("rf,df->rd", hidden, down_w, preferred_element_type=jnp.float32)
            total = part if total is None else total + part
    routed = lax.psum_scatter(
        total.astype(jnp.bfloat16), "fs", scatter_dimension=0, tiled=True
    )
    routed = lax.all_to_all(routed, "tp", split_axis=1, concat_axis=0, tiled=True)
    layer_output = (routed.astype(jnp.float32) + shared_sum).astype(jnp.bfloat16)
    return (layer_output, sample_gate, sample_up, sample_down, common_gate, common_up, common_down)


def solution(mesh):
    return jax.shard_map(
        body,
        mesh=mesh,
        in_specs=(
            P("fs", None),
            P("fs", None),
            P("fs", None),
            P("fs"),
            P(None, "fs", "tp"),
            P(None, "fs", "tp"),
            P(None, "fs", "tp"),
            P("fs", "tp"),
            P("fs", "tp"),
            P("fs", "tp"),
        ),
        out_specs=(
            P("fs", "tp"),
            P("fs", None, "tp"),
            P("fs", None, "tp"),
            P("fs", None, "tp"),
            P(None, "tp"),
            P(None, "tp"),
            P(None, "tp"),
        ),
        check_vma=False,
    )
```

time: 620 us -> 609 us (0.982)
  local copies, waits for them, and re-layouts: 66.9 us -> 15.9 us
  matrix products: 39 us -> 62.8 us
  blocking collectives: 57 us -> 77.6 us
  waiting for transfers between devices: 343 us -> 363 us
  other arithmetic: 38.9 us -> 20.1 us
  starting transfers between devices: 59.8 us -> 52.8 us
    reduce_scatter x1, waiting for transfers between devices: 7.35 us -> 165 us  [body(): lax.psum_scatter(total.astype(jnp.bfloat16), 'fs', scatter_dimension=0, t...]
    all_gather x6 -> x4, waiting for transfers between devices: 183 us -> 61.1 us  [the longest x1 61.1 us: body(): lax.all_gather(shared_down.astype(jnp.bfloat16), 'fs', axis=0, tiled=True)]
    all_gather x0 -> x1, blocking collectives: none -> 73.4 us  [body(): dense_all = lax.all_gather(dense, 'fs', axis=0, tiled=False)]
    all_to_all x1, blocking collectives: 57 us -> 4.15 us  [body(): lax.all_to_all(routed, 'tp', split_axis=1, concat_axis=0, tiled=True)]
    all_to_all x2, starting transfers between devices: 45.6 us -> 12.1 us  [the longest x1 8.47 us: body(): lax.all_to_all(rounded[0], 'fs', split_axis=0, concat_axis=1, tiled=True)]
    all_to_all x2, waiting for transfers between devices: 99.7 us -> 67.5 us  [the longest x1 65.4 us: body(): lax.all_to_all(rounded[0], 'fs', split_axis=0, concat_axis=1, tiled=True)]
    all_to_all x1, waiting for transfers between devices: 38.7 us -> 68.5 us  [body(): lax.all_to_all(rounded[1], 'fs', split_axis=0, concat_axis=1, tiled=True)]
    gather x2 -> x0, local copies, waits for them, and re-layouts: 26.9 us -> none  [the longest x1 16.1 us: body(): taken = back[local].astype(jnp.float32).reshape(tok_rows, picks, width)]
  transfers between devices with their start and end apart: 11 -> 12, of which waited for: 6 -> 5; matrix products, arithmetic and copies ran while one was open for 14% -> 13% of each run, Pallas kernels for 0% -> 0%
where the time goes in v1:
time: 609 us; the launch traced here: 606 us
  waiting for transfers between devices  363 us (60%)
  blocking collectives  77.6 us (13%)
  matrix products  62.8 us (10%)
  starting transfers between devices  52.8 us (9%)
  other arithmetic  20.1 us (3%)
  local copies, waits for them, and re-layouts  15.9 us (3%)
  between operations  14 us (2%)
    reduce_scatter x1, waiting for transfers between devices, body(): lax.psum_scatter(total.astype(jnp.bfloat16), 'fs', scatter_dimension=0, t...  165 us
    all_gather x1, blocking collectives, body(): dense_all = lax.all_gather(dense, 'fs', axis=0, tiled=False)  73.4 us
    all_to_all x1, waiting for transfers between devices, body(): lax.all_to_all(rounded[1], 'fs', split_axis=0, concat_axis=1, tiled=True)  68.5 us
    all_to_all x1, waiting for transfers between devices, body(): lax.all_to_all(rounded[0], 'fs', split_axis=0, concat_axis=1, tiled=True)  65.4 us
    all_gather x1, waiting for transfers between devices, body(): lax.all_gather(shared_down.astype(jnp.bfloat16), 'fs', axis=0, tiled=True)  61.1 us
    dot_general x2, matrix products, body(): jnp.einsum('rf,df->rd', hidden, down_w, preferred_element_type=jnp.float32)  30.2 us
    all_to_all x1, starting transfers between devices, body(): lax.all_to_all(rounded[2], 'fs', split_axis=0, concat_axis=1, tiled=True)  23.6 us
    dot_general x2, matrix products, body(): gate = jnp.dot(gathered, gate_w, preferred_element_type=jnp.float32)  17.3 us
  transfers between devices with their start and end apart: 12, of which 5 were waited for; matrix products, arithmetic and copies ran while one was open for 13% of the time, Pallas kernels for 0%

profile of v1, /device:TPU:0, one launch (start us, length us, event | category | flops | bytes accessed | tf_op | source)
XLA Modules:
  0.0 606.0 jit_solution(15371878558450184911)
XLA Ops:
  7.2 0.0 copy-start
  7.2 0.0 copy-start.8
  7.2 0.0 all-gather.6.cloned.1.call-start
  7.2 1.5 fusion
  8.8 1.5 fusion.1
  10.2 0.8 constant_dynamic-slice_fusion.3
  11.1 0.0 all-gather.6.cloned.1.call-update
  11.1 0.0 copy-done.8
  11.1 6.8 %multiply_convert_fusion.2 = (bf16[16,128,512]{2,1,0:T(8,128)(2,1)}, bf16[16,128,512]{2,1,0:T(8,128)(2,1)}) fusion(f32[16,128,512]{2,1,0:T(8,128)} %param.15, f32[128]{0:T(128)S(1)} %copy-done.8, f32[16,128,512]{2,1,0:T(8,128)} %param.14), kind=kLoop, calls=%fused_computation.3 | loop fusion | flops 4194304 | bytes 12583424 | tf_op jit(solution)/shard_map/convert_element_type | solution.py:47
  17.9 8.5 %all-to-all-start = ((bf16[16,128,512]{2,1,0:T(8,128)(2,1)}), bf16[16,128,512]{2,1,0:T(8,128)(2,1)S(1)}, u32[]{:S(2)}, u32[]{:S(2)}) async-start(bf16[16,128,512]{2,1,0:T(8,128)(2,1)} %get-tuple-element.8), calls=%async_computation | async-start | bytes 4194304 | tf_op jit(solution)/shard_map/all_to_all | solution.py:51
  26.4 0.0 all-gather.8.cloned.1.call-start
  26.5 0.0 copy-done.6
  26.5 1.8 multiply_convert_fusion.6
  28.2 0.0 all-gather.8.cloned.1.call-update
  28.3 65.4 %all-to-all-done = bf16[16,128,512]{2,1,0:T(8,128)(2,1)S(1)} async-done(((bf16[16,128,512]{2,1,0:T(8,128)(2,1)}), bf16[16,128,512]{2,1,0:T(8,128)(2,1)S(1)}, u32[]{:S(2)}, u32[]{:S(2)}) %all-to-all-start) | async-done | bytes 2097184 | tf_op jit(solution)/shard_map/all_to_all | solution.py:51
  93.7 16.3 %all-to-all-start.1 = ((bf16[16,128,512]{2,1,0:T(8,128)(2,1)}), bf16[16,128,512]{2,1,0:T(8,128)(2,1)}, u32[]{:S(2)}, u32[]{:S(2)}) async-start(bf16[16,128,512]{2,1,0:T(8,128)(2,1)} %get-tuple-element.7), calls=%async_computation.1 | async-start | bytes 4194304 | tf_op jit(solution)/shard_map/all_to_all | solution.py:52
  110.0 0.0 all-gather.10.cloned.1.call-start
  110.0 0.7 all-gather.10.cloned.1.call-update
  110.7 0.0 copy-start.5
  110.7 0.0 copy-start.7
  110.8 4.4 convert_element_type.59
  115.2 68.5 %all-to-all-done.1 = bf16[16,128,512]{2,1,0:T(8,128)(2,1)} async-done(((bf16[16,128,512]{2,1,0:T(8,128)(2,1)}), bf16[16,128,512]{2,1,0:T(8,128)(2,1)}, u32[]{:S(2)}, u32[]{:S(2)}) %all-to-all-start.1) | async-done | bytes 2097184 | tf_op jit(solution)/shard_map/all_to_all | solution.py:52
  183.7 23.6 %all-to-all-start.2 = ((bf16[16,128,512]{2,1,0:T(8,128)(2,1)}), bf16[16,128,512]{2,1,0:T(8,128)(2,1)}, u32[]{:S(2)}, u32[]{:S(2)}) async-start(bf16[16,128,512]{2,1,0:T(8,128)(2,1)} %convert_element_type.59), calls=%async_computation.2 | async-start | bytes 4194304 | tf_op jit(solution)/shard_map/all_to_all | solution.py:53
  207.3 0.0 all-gather.12.cloned.1.call-start
  207.3 0.1 collective-permute-start
  207.4 0.0 copy-done.5
  207.4 0.7 convert_element_type.68
  208.1 0.0 all-gather.12.cloned.1.call-update
  208.1 0.0 reduce-scatter.2.cloned.1.call-start
  208.2 0.0 copy-done
  208.2 0.0 copy-done.7
  208.2 73.4 %all-gather = f32[256,128]{1,0:T(8,128)S(1)} all-gather(f32[16,128]{1,0:T(8,128)S(1)} %select_reduce_fusion), channel_id=2, replica_groups=mesh['fs'=16,'tp'=2] {'fs'}, dimensions={0}, use_global_device_ids=true | all-gather | bytes 139264 | tf_op jit(solution)/shard_map/all_gather | solution.py:42
  281.7 0.1 collective-permute-start.1
  281.8 0.0 all-to-all-done.2
  281.8 0.5 collective-permute-start.2
  282.3 9.7 %fusion.16 = f32[2048,512]{1,0:T(8,128)} fusion(bf16[2048,2048]{1,0:T(8,128)(2,1)} %all-gather.6.cloned.1.call-done, bf16[2048,512]{1,0:T(8,128)(2,1)S(1)} %bitcast.41), kind=kOutput, calls=%fused_computation.38 | convolution fusion | flops 4294967296 | bytes 14680064 | tf_op jit(solution)/shard_map/dot_general | solution.py:95
  291.9 0.0 collective-permute-done
  291.9 0.0 copy-done.9
  291.9 7.6 %fusion.17 = f32[2048,512]{1,0:T(8,128)} fusion(bf16[2048,2048]{1,0:T(8,128)(2,1)S(1)} %copy-done.9, bf16[2048,512]{1,0:T(8,128)(2,1)} %collective-permute-done), kind=kOutput, calls=%fused_computation.39 | convolution fusion | flops 4294967296 | bytes 14680064 | tf_op jit(solution)/shard_map/dot_general | solution.py:95
  299.6 0.0 collective-permute-done.1
  299.6 7.6 %fusion.18 = f32[2048,512]{1,0:T(8,128)} fusion(bf16[2048,2048]{1,0:T(8,128)(2,1)S(1)} %copy-done.9, bf16[2048,512]{1,0:T(8,128)(2,1)} %collective-permute-done.1), kind=kOutput, calls=%fused_computation.40 | convolution fusion | flops 4294967296 | bytes 14680064 | tf_op jit(solution)/shard_map/dot_general | solution.py:96
  307.1 16.6 %fusion.6 = f32[2048,2048]{1,0:T(8,128)} fusion(bf16[2048,512]{1,0:T(8,128)(2,1)} %bitcast.4, f32[2048,512]{1,0:T(8,128)} %fusion.16, bf16[2048,2048]{1,0:T(8,128)(2,1)} %all-gather.6.cloned.1.call-done, bf16[2048,512]{1,0:T(8,128)(2,1)} %bitcast.1, f32[2048]{0:T(1024)S(1)} %bitcast.48), kind=kOutput, calls=%fused_computation.18 | convolution fusion | flops 8597274624 | bytes 33562624 | tf_op jit(solution)/shard_map/rf,df->rd/dot_general | solution.py:98
  323.8 0.0 collective-permute-done.2
  323.8 13.5 %add_convert_fusion = bf16[2048,2048]{1,0:T(8,128)(2,1)} fusion(f32[2048,2048]{1,0:T(8,128)} %fusion.6, bf16[2048,512]{1,0:T(8,128)(2,1)} %collective-permute-done.2, f32[2048,512]{1,0:T(8,128)} %fusion.18, f32[2048,512]{1,0:T(8,128)} %fusion.17, f32[2048]{0:T(1024)S(1)} %bitcast.49), kind=kOutput, calls=%fused_computation | convolution fusion | flops 4310695936 | bytes 35659776 | tf_op jit(solution)/shard_map/rf,df->rd/dot_general | solution.py:98
  337.3 0.0 reduce-scatter.2.cloned.1.call-update
  337.3 0.0 all-gather.8.cloned.1.call-done
  337.4 3.1 fusion.19
  340.5 61.1 %all-gather.12.cloned.1.call-done = bf16[2048,512]{1,0:T(8,128)(2,1)} async-done(((bf16[128,512]{1,0:T(8,128)(2,1)}), bf16[2048,512]{1,0:T(8,128)(2,1)}) %all-gather.12.cloned.1.call-update) | async-done | bytes 2097168 | tf_op jit(solution)/shard_map/all_gather | solution.py:59
  401.5 4.7 convolution_convert_fusion
  406.2 2.3 copy.30
  408.5 3.6 all-to-all-start.4
  412.1 2.1 all-to-all-done.4
  414.2 1.2 convert_reduce_fusion
  415.4 165.0 %reduce-scatter.2.cloned.1.call-done = bf16[128,2048]{1,0:T(8,128)(2,1)} async-done(((bf16[2048,2048]{1,0:T(8,128)(2,1)}), bf16[128,2048]{1,0:T(8,128)(2,1)}) %reduce-scatter.2.cloned.1.call-update) | async-done | bytes 524304 | tf_op jit(solution)/shard_map/reduce_scatter | solution.py:100
  580.3 1.1 copy.31
  581.4 4.2 all_to_all.54
  585.6 2.2 fusion.5
  587.8 1.3 copy.38
  589.1 3.2 copy.39
  592.3 3.2 copy.40
  595.5 1.3 copy.41
  596.8 0.0 copy-done.3
  596.8 1.3 copy.42
  598.1 1.3 copy.43
  (16 shorter events, 0.1 us)
Async XLA Ops:
  7.2 201.0 %copy-start = (f32[256,6]{0,1:T(8,128)S(1)}, f32[256,6]{0,1:T(8,128)}, u32[]{:S(2)}) copy-start(f32[256,6]{0,1:T(8,128)} %param.12) | copy-start | bytes 18436
  7.2 3.9 copy-start.8
  7.2 275.1 %all-gather.6.cloned.1.call-start = ((), (), s32[]{:S(2)}) async-start(), calls=%async_computation.6 | async-start | bytes 8912896 | tf_op jit(solution)/shard_map/all_gather | solution.py:41
  17.9 8.5 %copy-start.6 = (f32[128,512]{1,0:T(8,128)S(1)}, f32[128,512]{1,0:T(8,128)}, u32[]{:S(2)}) copy-start(f32[128,512]{1,0:T(8,128)} %param.17) | copy-start | bytes 786436
  17.9 75.8 %all-to-all-start = ((bf16[16,128,512]{2,1,0:T(8,128)(2,1)}), bf16[16,128,512]{2,1,0:T(8,128)(2,1)S(1)}, u32[]{:S(2)}, u32[]{:S(2)}) async-start(bf16[16,128,512]{2,1,0:T(8,128)(2,1)} %get-tuple-element.8), calls=%async_computation | async-start | bytes 4194304 | tf_op jit(solution)/shard_map/all_to_all | solution.py:51
  26.4 310.9 %all-gather.8.cloned.1.call-start = ((), (), s32[]{:S(2)}) async-start(), calls=%async_computation.8 | async-start | bytes 2228224 | tf_op jit(solution)/shard_map/all_gather | solution.py:57
  93.7 90.0 %all-to-all-start.1 = ((bf16[16,128,512]{2,1,0:T(8,128)(2,1)}), bf16[16,128,512]{2,1,0:T(8,128)(2,1)}, u32[]{:S(2)}, u32[]{:S(2)}) async-start(bf16[16,128,512]{2,1,0:T(8,128)(2,1)} %get-tuple-element.7), calls=%async_computation.1 | async-start | bytes 4194304 | tf_op jit(solution)/shard_map/all_to_all | solution.py:52
  110.0 230.5 %all-gather.10.cloned.1.call-start = ((), (), s32[]{:S(2)}) async-start(), calls=%async_computation.9 | async-start | bytes 2228224 | tf_op jit(solution)/shard_map/all_gather | solution.py:58
  110.7 96.7 %copy-start.5 = (f32[128,512]{1,0:T(8,128)S(1)}, f32[128,512]{1,0:T(8,128)}, u32[]{:S(2)}) copy-start(f32[128,512]{1,0:T(8,128)} %param.19) | copy-start | bytes 786436
  110.7 97.4 %copy-start.7 = (s32[256,6]{0,1:T(8,128)S(1)}, s32[256,6]{0,1:T(8,128)}, u32[]{:S(2)}) copy-start(s32[256,6]{0,1:T(8,128)} %param.11) | copy-start | bytes 18436
  183.7 98.1 %all-to-all-start.2 = ((bf16[16,128,512]{2,1,0:T(8,128)(2,1)}), bf16[16,128,512]{2,1,0:T(8,128)(2,1)}, u32[]{:S(2)}, u32[]{:S(2)}) async-start(bf16[16,128,512]{2,1,0:T(8,128)(2,1)} %convert_element_type.59), calls=%async_computation.2 | async-start | bytes 4194304 | tf_op jit(solution)/shard_map/all_to_all | solution.py:53
  207.3 194.2 %all-gather.12.cloned.1.call-start = ((), (), s32[]{:S(2)}) async-start(), calls=%async_computation.10 | async-start | bytes 2228224 | tf_op jit(solution)/shard_map/all_gather | solution.py:59
  207.3 84.6 %collective-permute-start = (bf16[2048,512]{1,0:T(8,128)(2,1)S(1)}, bf16[2048,512]{1,0:T(8,128)(2,1)}, u32[]{:S(2)}, u32[]{:S(2)}) collective-permute-start(bf16[2048,512]{1,0:T(8,128)(2,1)S(1)} %bitcast.40), channel_id=1, source_target_pairs={{0,1},{1,0},{2,3},{3,2},{4,5},{5,4},{6,7},{7,6},{8,9},{9,8},{10,11... | collective-permute-start | bytes 6291464 | tf_op jit(solution)/shard_map/ppermute | solution.py:91
  208.1 372.2 %reduce-scatter.2.cloned.1.call-start = ((), (), s32[]{:S(2)}) async-start(), calls=%async_computation.7 | async-start | bytes 8912896 | tf_op jit(solution)/shard_map/reduce_scatter | solution.py:100
  281.7 17.9 %collective-permute-start.1 = (bf16[2048,512]{1,0:T(8,128)(2,1)}, bf16[2048,512]{1,0:T(8,128)(2,1)}, u32[]{:S(2)}, u32[]{:S(2)}) collective-permute-start(bf16[2048,512]{1,0:T(8,128)(2,1)} %bitcast.1), channel_id=1, source_target_pairs={{0,1},{1,0},{2,3},{3,2},{4,5},{5,4},{6,7},{7,6},{8,9},{9,8},{10,11... | collective-permute-start | bytes 6291464 | tf_op jit(solution)/shard_map/ppermute | solution.py:92
  281.8 42.0 %collective-permute-start.2 = (bf16[2048,512]{1,0:T(8,128)(2,1)}, bf16[2048,512]{1,0:T(8,128)(2,1)}, u32[]{:S(2)}, u32[]{:S(2)}) collective-permute-start(bf16[2048,512]{1,0:T(8,128)(2,1)} %bitcast.4), channel_id=1, source_target_pairs={{0,1},{1,0},{2,3},{3,2},{4,5},{5,4},{6,7},{7,6},{8,9},{9,8},{10,11... | collective-permute-start | bytes 6291464 | tf_op jit(solution)/shard_map/ppermute | solution.py:93
  282.3 9.7 %copy-start.9 = (bf16[2048,2048]{1,0:T(8,128)(2,1)S(1)}, bf16[2048,2048]{1,0:T(8,128)(2,1)}, u32[]{:S(2)}) copy-start(bf16[2048,2048]{1,0:T(8,128)(2,1)} %all-gather.6.cloned.1.call-done) | copy-start | bytes 25165828
  408.5 5.7 all-to-all-start.4
  589.1 6.4 %copy-start.2 = (bf16[2048,512]{1,0:T(8,128)(2,1)S(1)}, bf16[2048,512]{1,0:T(8,128)(2,1)}, u32[]{:S(2)}) copy-start(bf16[2048,512]{1,0:T(8,128)(2,1)} %all-gather.8.cloned.1.call-done) | copy-start | bytes 6291460
  592.3 4.5 copy-start.3
  595.5 2.6 copy-start.4
  595.5 4.0 copy-start.1
Sparse Core Ops, SparseCore 0:
  11.3 191.9 all-gather.5
  206.7 69.6 all-gather.7
  279.8 59.2 all-gather.9
  342.3 59.1 all-gather.11
  403.7 176.6 reduce-scatter.1

commit v2 on v1

--- a/solution.py
+++ b/solution.py
@@ -10,6 +10,22 @@
     values = tokens.astype(jnp.float32)
     scale = lax.rsqrt(jnp.mean(values * values, axis=-1, keepdims=True) + EPSILON)
     return (values * scale).astype(jnp.bfloat16)
+
+
+def ring_of(fs_count):
+    if fs_count != 16:
+        return list(range(fs_count))
+    order = []
+    for place, column in enumerate((0, 1, 3, 2)):
+        heights = range(4) if place % 2 == 0 else range(3, -1, -1)
+        order.extend(height * 4 + column for height in heights)
+    return order
+
+
+def reorder(blocks, order):
+    if list(order) == list(range(len(order))):
+        return blocks
+    return jnp.concatenate([blocks[i : i + 1] for i in order], axis=0)
 
 
 def body(
@@ -31,6 +47,9 @@
     experts = expert_gate.shape[0]
     share = tok_rows // tp_count
     own_experts = experts // fs_count
+    ring = ring_of(fs_count)
+    place_of = [ring.index(i) for i in range(fs_count)]
+    groups = None if ring == list(range(fs_count)) else [ring]
 
     normed = normalize(tokens)
     own_normed = lax.dynamic_slice_in_dim(normed, tp_index * share, share, 0)
@@ -38,8 +57,10 @@
     own_weights = lax.dynamic_slice_in_dim(route_weights, tp_index * share, share, 0)
     member = own_routes[None, :, :] == jnp.arange(experts, dtype=jnp.int32)[:, None, None]
     dense = jnp.sum(jnp.where(member, own_weights[None, :, :], 0.0), axis=2)
-    gathered = lax.all_gather(own_normed, "fs", axis=0, tiled=True)
     dense_all = lax.all_gather(dense, "fs", axis=0, tiled=False)
+    own_normed, dense_all = lax.optimization_barrier((own_normed, dense_all))
+    gathered = lax.all_gather(own_normed, "fs", axis=0, tiled=False)
+    gathered = reorder(gathered, ring).reshape(fs_count * share, width)
 
     gain_rows = norm_gain[None, :, None]
     rounded = (
@@ -53,10 +74,19 @@
         lax.all_to_all(rounded[2], "fs", split_axis=0, concat_axis=1, tiled=True),
     )
 
+    half = shared_gate.shape[1]
+    shared_rows = jnp.concatenate(
+        [
+            (shared_gate * norm_gain[:, None]).astype(jnp.bfloat16),
+            (shared_up * norm_gain[:, None]).astype(jnp.bfloat16),
+            shared_down.astype(jnp.bfloat16),
+        ],
+        axis=1,
+    )
+    common = lax.all_gather(shared_rows, "fs", axis=0, tiled=False, axis_index_groups=groups)
     common_gate, common_up, common_down = (
-        lax.all_gather((shared_gate * norm_gain[:, None]).astype(jnp.bfloat16), "fs", axis=0, tiled=True),
-        lax.all_gather((shared_up * norm_gain[:, None]).astype(jnp.bfloat16), "fs", axis=0, tiled=True),
-        lax.all_gather(shared_down.astype(jnp.bfloat16), "fs", axis=0, tiled=True),
+        reorder(common[:, :, i * half : (i + 1) * half], place_of).reshape(width, half)
+        for i in range(3)
     )
     shared_gate_act = jnp.dot(normed, common_gate, preferred_element_type=jnp.float32)
     shared_up_act = jnp.dot(normed, common_up, preferred_element_type=jnp.float32)
@@ -73,8 +103,11 @@
     )
     shared_sum = jnp.sum(shared_parts.astype(jnp.float32), axis=0)
 
-    scale_all = lax.dynamic_slice_in_dim(
-        dense_all, lax.axis_index("fs") * own_experts, own_experts, 1
+    scale_all = reorder(
+        lax.dynamic_slice_in_dim(
+            dense_all, lax.axis_index("fs") * own_experts, own_experts, 1
+        ),
+        ring,
     )
     total = None
     for expert in range(own_experts):
@@ -86,11 +119,11 @@
                 sample_down[expert],
             )
             if shift:
-                ring = [(i, (i + shift) % tp_count) for i in range(tp_count)]
+                pairs = [(i, (i + shift) % tp_count) for i in range(tp_count)]
                 gate_w, up_w, down_w = (
-                    lax.ppermute(gate_w, "tp", ring),
-                    lax.ppermute(up_w, "tp", ring),
-                    lax.ppermute(down_w, "tp", ring),
+                    lax.ppermute(gate_w, "tp", pairs),
+                    lax.ppermute(up_w, "tp", pairs),
+                    lax.ppermute(down_w, "tp", pairs),
                 )
             gate = jnp.dot(gathered, gate_w, preferred_element_type=jnp.float32)
             upward = jnp.dot(gathered, up_w, preferred_element_type=jnp.float32)
@@ -98,7 +131,7 @@
             part = jnp.einsum("rf,df->rd", hidden, down_w, preferred_element_type=jnp.float32)
             total = part if total is None else total + part
     routed = lax.psum_scatter(
-        total.astype(jnp.bfloat16), "fs", scatter_dimension=0, tiled=True
+        total.astype(jnp.bfloat16), "fs", scatter_dimension=0, tiled=True, axis_index_groups=groups
     )
     routed = lax.all_to_all(routed, "tp", split_axis=1, concat_axis=0, tiled=True)
     layer_output = (routed.astype(jnp.float32) + shared_sum).astype(jnp.bfloat16)

time: 609 us -> 482 us (0.79)
  waiting for transfers between devices: 363 us -> 198 us
  blocking collectives: 77.6 us -> 130 us
  starting transfers between devices: 52.8 us -> 27.9 us
  local copies, waits for them, and re-layouts: 15.9 us -> 37.5 us
    reduce_scatter x1, waiting for transfers between devices: 165 us -> 71.9 us  [body(): lax.psum_scatter(total.astype(jnp.bfloat16), 'fs', scatter_dimension=0, t...]
    all_to_all x0 -> x2, blocking collectives: none -> 82.8 us  [the longest x1 78.2 us: body(): lax.all_to_all(rounded[0], 'fs', split_axis=0, concat_axis=1, tiled=True)]
    all_to_all x2 -> x0, waiting for transfers between devices: 67.5 us -> none  [the longest x1 65.4 us: body(): lax.all_to_all(rounded[0], 'fs', split_axis=0, concat_axis=1, tiled=True)]
    all_gather x4 -> x2, waiting for transfers between devices: 61.1 us -> 0.02 us  [the longest x1 0.02 us: body(): lax.all_gather(shared_rows, 'fs', axis=0, tiled=False, axis_index_groups=...]
    all_to_all x1, waiting for transfers between devices: 0.01 us -> 57.3 us  [body(): lax.all_to_all(rounded[2], 'fs', split_axis=0, concat_axis=1, tiled=True)]
    all_gather x1, blocking collectives: 73.4 us -> 43.1 us  [body(): dense_all = lax.all_gather(dense, 'fs', axis=0, tiled=False)]
    unnamed x26 -> x63, local copies, waits for them, and re-layouts: 11.7 us -> 32.5 us
    all_to_all x2 -> x0, starting transfers between devices: 12.1 us -> none  [the longest x1 8.47 us: body(): lax.all_to_all(rounded[0], 'fs', split_axis=0, concat_axis=1, tiled=True)]
  transfers between devices with their start and end apart: 12 -> 8, of which waited for: 5 -> 3; matrix products, arithmetic and copies ran while one was open for 13% -> 20% of each run, Pallas kernels for 0% -> 0%
where the time goes in v2:
time: 482 us; the launch traced here: 481 us
  waiting for transfers between devices  198 us (41%)
  blocking collectives  130 us (27%)
  matrix products  57.7 us (12%)
  local copies, waits for them, and re-layouts  37.5 us (8%)
  starting transfers between devices  27.9 us (6%)
  other arithmetic  16 us (3%)
  between operations  14.1 us (3%)
    all_to_all x1, blocking collectives, body(): lax.all_to_all(rounded[0], 'fs', split_axis=0, concat_axis=1, tiled=True)  78.2 us
    reduce_scatter x1, waiting for transfers between devices, body(): lax.psum_scatter(total.astype(jnp.bfloat16), 'fs', scatter_dimension=0, t...  71.9 us
    all_to_all x1, waiting for transfers between devices, body(): lax.all_to_all(rounded[1], 'fs', split_axis=0, concat_axis=1, tiled=True)  68.6 us
    all_to_all x1, waiting for transfers between devices, body(): lax.all_to_all(rounded[2], 'fs', split_axis=0, concat_axis=1, tiled=True)  57.3 us
    all_gather x1, blocking collectives, body(): dense_all = lax.all_gather(dense, 'fs', axis=0, tiled=False)  43.1 us
    unnamed x63, local copies, waits for them, and re-layouts  32.5 us
    dot_general x2, matrix products, body(): jnp.einsum('rf,df->rd', hidden, down_w, preferred_element_type=jnp.float32)  30.2 us
    all_to_all x1, starting transfers between devices, body(): lax.all_to_all(rounded[2], 'fs', split_axis=0, concat_axis=1, tiled=True)  22.6 us
  transfers between devices with their start and end apart: 8, of which 3 were waited for; matrix products, arithmetic and copies ran while one was open for 20% of the time, Pallas kernels for 0%

profile of v2, /device:TPU:0, one launch (start us, length us, event | category | flops | bytes accessed | tf_op | source)
XLA Modules:
  0.0 481.2 jit_solution(11208492477389067535)
XLA Ops:
  7.2 0.0 all-gather.6.cloned.1.call-start
  7.2 0.6 copy-done
  7.9 0.7 constant_dynamic-slice_fusion.16
  8.6 43.1 %all-gather = f32[256,128]{1,0:T(8,128)S(1)} all-gather(f32[16,128]{1,0:T(8,128)S(1)} %select_reduce_fusion), channel_id=2, replica_groups=mesh['fs'=16,'tp'=2] {'fs'}, dimensions={0}, use_global_device_ids=true | all-gather | bytes 139264 | tf_op jit(solution)/shard_map/all_gather | solution.py:60
  51.7 1.5 fusion
  53.2 1.5 fusion.1
  54.7 0.8 constant_dynamic-slice_fusion.17
  55.5 0.0 all-gather.6.cloned.1.call-update
  55.5 6.1 %multiply_convert_fusion.2 = (bf16[16,128,512]{2,1,0:T(8,128)(2,1)}, bf16[16,128,512]{2,1,0:T(8,128)(2,1)S(1)}) fusion(f32[16,128,512]{2,1,0:T(8,128)} %param.15, f32[128]{0:T(128)S(1)} %copy-done.8, f32[16,128,512]{2,1,0:T(8,128)} %param.14), kind=kLoop, calls=%fused_computation.3 | loop fusion | flops 4194304 | bytes 12583424 | tf_op jit(solution)/shard_map/convert_element_type | solution.py:68
  61.7 78.2 %all_to_all.54 = bf16[16,128,512]{2,1,0:T(8,128)(2,1)S(1)} all-to-all(bf16[16,128,512]{2,1,0:T(8,128)(2,1)S(1)} %get-tuple-element.57), channel_id=1, replica_groups=mesh['fs'=16,'tp'=2] {'fs'}, dimensions={0} | all-to-all | bytes 4194304 | tf_op jit(solution)/shard_map/all_to_all | solution.py:72
  139.9 4.5 all-to-all-start.1
  144.4 3.8 convert_element_type.59
  148.2 68.6 %all-to-all-done.1 = bf16[16,128,512]{2,1,0:T(8,128)(2,1)} async-done(((bf16[16,128,512]{2,1,0:T(8,128)(2,1)}), bf16[16,128,512]{2,1,0:T(8,128)(2,1)}, u32[]{:S(2)}, u32[]{:S(2)}) %all-to-all-start.1) | async-done | bytes 2097184 | tf_op jit(solution)/shard_map/all_to_all | solution.py:73
  216.8 22.6 %all-to-all-start.2 = ((bf16[16,128,512]{2,1,0:T(8,128)(2,1)}), bf16[16,128,512]{2,1,0:T(8,128)(2,1)}, u32[]{:S(2)}, u32[]{:S(2)}) async-start(bf16[16,128,512]{2,1,0:T(8,128)(2,1)} %convert_element_type.59), calls=%async_computation.2 | async-start | bytes 4194304 | tf_op jit(solution)/shard_map/all_to_all | solution.py:74
  239.4 0.0 all-gather.8.cloned.1.call-start
  239.4 1.1 multiply_convert_fusion.6
  240.6 0.8 pad_maximum_fusion
  241.3 0.0 all-gather.8.cloned.1.call-update
  241.4 0.2 reduce-scatter.2.cloned.1.call-start
  241.9 0.1 collective-permute-start
  242.0 0.5 collective-permute-start.1
  242.5 57.3 %all-to-all-done.2 = bf16[16,128,512]{2,1,0:T(8,128)(2,1)} async-done(((bf16[16,128,512]{2,1,0:T(8,128)(2,1)}), bf16[16,128,512]{2,1,0:T(8,128)(2,1)}, u32[]{:S(2)}, u32[]{:S(2)}) %all-to-all-start.2) | async-done | bytes 2097184 | tf_op jit(solution)/shard_map/all_to_all | solution.py:74
  299.8 1.1 fusion.20
  300.9 1.2 fusion.19
  302.1 1.8 fusion.18
  303.9 0.1 constant_dynamic-update-slice_fusion
  304.0 1.1 fusion.17
  305.1 1.1 fusion.16
  306.2 1.1 fusion.15
  307.7 6.0 %fusion.30 = f32[2048,512]{1,0:T(8,128)} fusion(bf16[2048,2048]{1,0:T(8,128)(2,1)S(1)} %bitcast.140, bf16[2048,512]{1,0:T(8,128)(2,1)S(1)} %bitcast.104), kind=kOutput, calls=%fused_computation.142 | convolution fusion | flops 4294967296 | bytes 14680064 | tf_op jit(solution)/shard_map/dot_general | solution.py:128
  313.7 7.6 %fusion.31 = f32[2048,512]{1,0:T(8,128)} fusion(bf16[2048,2048]{1,0:T(8,128)(2,1)S(1)} %bitcast.141, bf16[2048,512]{1,0:T(8,128)(2,1)} %collective-permute-done), kind=kOutput, calls=%fused_computation.143 | convolution fusion | flops 4294967296 | bytes 14680064 | tf_op jit(solution)/shard_map/dot_general | solution.py:128
  321.3 7.6 %fusion.32 = f32[2048,512]{1,0:T(8,128)} fusion(bf16[2048,2048]{1,0:T(8,128)(2,1)S(1)} %bitcast.142, bf16[2048,512]{1,0:T(8,128)(2,1)} %collective-permute-done.1), kind=kOutput, calls=%fused_computation.144 | convolution fusion | flops 4294967296 | bytes 14680064 | tf_op jit(solution)/shard_map/dot_general | solution.py:129
  328.9 16.7 %fusion.6 = f32[2048,2048]{1,0:T(8,128)} fusion(bf16[2048,512]{1,0:T(8,128)(2,1)} %bitcast.20, f32[2048,512]{1,0:T(8,128)} %fusion.30, bf16[2048,2048]{1,0:T(8,128)(2,1)} %bitcast.143, bf16[2048,512]{1,0:T(8,128)(2,1)} %bitcast.18, f32[2048]{0:T(1024)S(1)} %bitcast.150), kind=kOutput, calls=%fused_computation.18 | convolution fusion | flops 8597274624 | bytes 33562624 | tf_op jit(solution)/shard_map/rf,df->rd/dot_general | solution.py:131
  345.6 13.5 %add_convert_fusion = bf16[2048,2048]{1,0:T(8,128)(2,1)} fusion(f32[2048,2048]{1,0:T(8,128)} %fusion.6, bf16[2048,512]{1,0:T(8,128)(2,1)} %collective-permute-done.2, f32[2048,512]{1,0:T(8,128)} %fusion.32, f32[2048,512]{1,0:T(8,128)} %fusion.31, f32[2048]{0:T(1024)S(1)} %bitcast.151), kind=kOutput, calls=%fused_computation | convolution fusion | flops 4310695936 | bytes 35659776 | tf_op jit(solution)/shard_map/rf,df->rd/dot_general | solution.py:131
  359.1 0.0 reduce-scatter.2.cloned.1.call-update
  359.1 0.0 all-gather.8.cloned.1.call-done
  359.2 1.1 constant_dynamic-update-slice_fusion.29
  360.2 1.1 constant_dynamic-update-slice_fusion.28
  361.3 1.1 constant_dynamic-update-slice_fusion.27
  362.4 1.1 constant_dynamic-update-slice_fusion.26
  363.4 1.1 constant_dynamic-update-slice_fusion.25
  364.5 1.1 constant_dynamic-update-slice_fusion.24
  365.5 1.1 constant_dynamic-update-slice_fusion.23
  366.6 1.1 constant_dynamic-update-slice_fusion.22
  367.7 1.1 constant_dynamic-update-slice_fusion.21
  368.7 1.1 constant_dynamic-update-slice_fusion.20
  369.8 1.1 constant_dynamic-update-slice_fusion.19
  370.9 1.1 constant_dynamic-update-slice_fusion.18
  371.9 1.2 slice_dynamic-update-slice_fusion.2
  373.1 1.2 constant_dynamic-update-slice_fusion.17
  374.3 1.1 constant_dynamic-update-slice_fusion.16
  375.4 1.3 copy-done.5
  376.7 1.5 fusion.33
  378.2 4.8 convolution_convert_fusion
  383.0 1.3 copy.30
  384.3 4.6 all_to_all.55
  388.9 0.2 convert_reduce_fusion
  389.1 71.9 %reduce-scatter.2.cloned.1.call-done = bf16[128,2048]{1,0:T(8,128)(2,1)} async-done(((bf16[2048,2048]{1,0:T(8,128)(2,1)}), bf16[128,2048]{1,0:T(8,128)(2,1)}) %reduce-scatter.2.cloned.1.call-update) | async-done | bytes 524304 | tf_op jit(solution)/shard_map/reduce_scatter | solution.py:133
  461.0 1.1 copy.31
  462.1 4.2 all_to_all.56
  466.3 0.9 fusion.5
  467.2 1.3 copy.105
  468.5 3.1 copy.106
  471.6 3.0 copy.107
  (50 shorter events, 0.7 us)
Async XLA Ops:
  7.2 0.7 copy-start
  7.2 292.6 %all-gather.6.cloned.1.call-start = ((), (), s32[]{:S(2)}) async-start(), calls=%async_computation.7 | async-start | bytes 8912896 | tf_op jit(solution)/shard_map/all_gather | solution.py:62
  53.2 2.4 copy-start.8
  139.9 76.9 %all-to-all-start.1 = ((bf16[16,128,512]{2,1,0:T(8,128)(2,1)}), bf16[16,128,512]{2,1,0:T(8,128)(2,1)}, u32[]{:S(2)}, u32[]{:S(2)}) async-start(bf16[16,128,512]{2,1,0:T(8,128)(2,1)} %get-tuple-element.56), calls=%async_computation.1 | async-start | bytes 4194304 | tf_op jit(solution)/shard_map/all_to_all | solution.py:73
  148.2 91.2 %copy-start.3 = (f32[128,512]{1,0:T(8,128)S(1)}, f32[128,512]{1,0:T(8,128)}, u32[]{:S(2)}) copy-start(f32[128,512]{1,0:T(8,128)} %param.19) | copy-start | bytes 786436
  216.8 83.0 %all-to-all-start.2 = ((bf16[16,128,512]{2,1,0:T(8,128)(2,1)}), bf16[16,128,512]{2,1,0:T(8,128)(2,1)}, u32[]{:S(2)}, u32[]{:S(2)}) async-start(bf16[16,128,512]{2,1,0:T(8,128)(2,1)} %convert_element_type.59), calls=%async_computation.2 | async-start | bytes 4194304 | tf_op jit(solution)/shard_map/all_to_all | solution.py:74
  239.4 119.8 %all-gather.8.cloned.1.call-start = ((), (), s32[]{:S(2)}) async-start(), calls=%async_computation.8 | async-start | bytes 6684672 | tf_op jit(solution)/shard_map/all_gather | solution.py:86
  241.4 219.7 %reduce-scatter.2.cloned.1.call-start = ((), (), s32[]{:S(2)}) async-start(), calls=%async_computation.6 | async-start | bytes 8912896 | tf_op jit(solution)/shard_map/reduce_scatter | solution.py:133
  241.9 71.8 %collective-permute-start = (bf16[2048,512]{1,0:T(8,128)(2,1)S(1)}, bf16[2048,512]{1,0:T(8,128)(2,1)}, u32[]{:S(2)}, u32[]{:S(2)}) collective-permute-start(bf16[2048,512]{1,0:T(8,128)(2,1)S(1)} %bitcast.103), channel_id=1, source_target_pairs={{0,1},{1,0},{2,3},{3,2},{4,5},{5,4},{6,7},{7,6},{8,9},{9,8},{10,11... | collective-permute-start | bytes 6291464 | tf_op jit(solution)/shard_map/ppermute | solution.py:124
  242.0 79.3 %collective-permute-start.1 = (bf16[2048,512]{1,0:T(8,128)(2,1)}, bf16[2048,512]{1,0:T(8,128)(2,1)}, u32[]{:S(2)}, u32[]{:S(2)}) collective-permute-start(bf16[2048,512]{1,0:T(8,128)(2,1)} %bitcast.18), channel_id=1, source_target_pairs={{0,1},{1,0},{2,3},{3,2},{4,5},{5,4},{6,7},{7,6},{8,9},{9,8},{10,11... | collective-permute-start | bytes 6291464 | tf_op jit(solution)/shard_map/ppermute | solution.py:125
  299.8 45.8 %collective-permute-start.2 = (bf16[2048,512]{1,0:T(8,128)(2,1)}, bf16[2048,512]{1,0:T(8,128)(2,1)}, u32[]{:S(2)}, u32[]{:S(2)}) collective-permute-start(bf16[2048,512]{1,0:T(8,128)(2,1)} %bitcast.20), channel_id=1, source_target_pairs={{0,1},{1,0},{2,3},{3,2},{4,5},{5,4},{6,7},{7,6},{8,9},{9,8},{10,11... | collective-permute-start | bytes 6291464 | tf_op jit(solution)/shard_map/ppermute | solution.py:126
  300.8 3.1 slice-start
  300.8 6.4 %copy-start.2 = (bf16[2048,2048]{1,0:T(8,128)(2,1)S(1)}, bf16[2048,2048]{1,0:T(8,128)(2,1)}, u32[]{:S(2)}) copy-start(bf16[2048,2048]{1,0:T(8,128)(2,1)} %all-gather.6.cloned.1.call-done) | copy-start | bytes 25165828
  307.7 13.6 %copy-start.4 = (bf16[16,128,2048]{2,1,0:T(8,128)(2,1)}, bf16[16,128,2048]{2,1,0:T(8,128)(2,1)S(1)}, u32[]{:S(2)}) copy-start(bf16[16,128,2048]{2,1,0:T(8,128)(2,1)S(1)} %fusion.7) | copy-start | bytes 25165828
  375.4 1.3 copy-start.5
  375.4 2.8 copy-start.6
  375.4 2.8 copy-start.7
  468.5 6.1 %copy-start.1 = (f32[256,6]{0,1:T(8,128)S(1)}, f32[256,6]{0,1:T(8,128)}, u32[]{:S(2)}) copy-start(f32[256,6]{0,1:T(8,128)} %param.12) | copy-start | bytes 18436
Sparse Core Ops, SparseCore 0:
  55.7 179.2 all-gather.5
  242.3 108.1 all-gather.7
  359.2 101.7 reduce-scatter.1
